TPU v7x, 32 devices: a whole 2x2x4 slice. The times are simulated.
32 devices in a mesh: sp: 8 (over z, y), tp: 4 (over x, core).
Axes of the slice: x: 2, y: 2, z: 4, core: 2. Of those that a mesh axis runs over, the one named last changes fastest.
Arguments:
- layer_input_rows: bfloat16 [2048, 2048], P('sp'), may hold values from -6 to 6
- input_norm_gain: float32 [2048], replicated, may hold values from 0.1 to 1.9
- query_weight: bfloat16 [2048, 1024], P(None, 'tp'), may hold values from -0.125 to 0.125
- key_weight: bfloat16 [2048, 1024], P(None, 'tp'), may hold values from -0.125 to 0.125
- value_weight: bfloat16 [2048, 1024], P(None, 'tp'), may hold values from -0.125 to 0.125
- query_norm_gain: float32 [64], replicated, may hold values from 0.5 to 9
- key_norm_gain: float32 [64], replicated, may hold values from 0.5 to 9
- cumulative_gate: float32 [2048, 16], P('sp', 'tp'), may hold values from -288.72 to 0, as said below
- attention_norm_gain: float32 [1024], P('tp'), may hold values from 0.1 to 1.9
- recurrence_query_weight: bfloat16 [2048, 1024], P(None, 'tp'), may hold values from -0.125 to 0.125
- forget_weight: bfloat16 [2048, 1024], P(None, 'tp'), may hold values from -0.125 to 0.125
- recurrence_value_weight: bfloat16 [2048, 1024], P(None, 'tp'), may hold values from -0.125 to 0.125
- output_gate_weight: bfloat16 [2048, 1024], P(None, 'tp'), may hold values from -0.125 to 0.125
- gate_lower_slack: float32 [1024], P('tp'), may hold values from 0 to 0.06
- extra_log_decay: float32 [2048, 8], P('sp', 'tp'), may hold values from -1.5 to 0
- recurrence_norm_gain: float32 [1024], P('tp'), may hold values from 0.1 to 1.9
- attention_output_weight: bfloat16 [1024, 2048], P('tp'), may hold values from -0.125 to 0.125
- recurrence_output_weight: bfloat16 [1024, 2048], P('tp'), may hold values from -0.125 to 0.125
Outputs:
- mixed: bfloat16 [2048, 2048], P(('sp', 'tp'))
- log_sum: float32 [2048, 16], P('sp', 'tp')
Inputs may be any that keep to these rules, and one draw needn't show every extreme that they name: `cumulative_gate`: each column never rises along positions.
All inputs are finite; a program needn't handle non-finite values.
Results may differ from a plain program's by a relative error of at most 0.015.
The roundings to bfloat16 on the way count: a program that leaves them out, or rounds other values in their place, can miss the bound.
Values may be sent and summed in bfloat16 or wider, within the bound.
A program may use at most 64 MiB of HBM per device.

v0:
```python
import math

import jax
import jax.numpy as jnp
from jax import lax
from jax.sharding import PartitionSpec as P

HEAD_DIM = 64
STATE_ROWS = 128
VAL_DIM = 128
BLOCK = 64


EPSILON = 1e-06
HIGHEST_ACCURACY = lax.Precision.HIGHEST


def entering(shard, axis, combine, identity):
    count, index = (lax.axis_size(axis), lax.axis_index(axis))
    everything = jax.tree.map(
        lambda part, kind: lax.all_gather(part.astype(kind), axis),
        shard,
        (jnp.bfloat16, jnp.bfloat16),
    )
    start = jax.tree.map(
        lambda part, zero: jnp.broadcast_to(jnp.asarray(zero, part.dtype), part.shape),
        shard,
        identity,
    )

    def step(k, before):
        reached = k < index
        new = combine(
            before, jax.tree.map(lambda part, own: part[k].astype(own.dtype), everything, shard)
        )
        return jax.tree.map(lambda a, b: jnp.where(reached, a, b), new, before)

    return lax.fori_loop(0, count, step, start)


def rms_rows(values, gain):
    squares = jnp.mean(values * values, axis=-1, keepdims=True)
    return values * lax.rsqrt(squares + EPSILON) * gain


def project(normalized_input, weight):
    return jnp.dot(normalized_input, weight, preferred_element_type=jnp.float32)


def recur_blocks(rec_query, forget_fraction, rec_value, decay_logarithm, states):
    length, head_number, keydim = rec_query.shape
    span_rows = BLOCK
    blocks = length // span_rows
    lower_tri = jnp.arange(span_rows)[:, None] >= jnp.arange(span_rows)[None, :]

    def to_blocks(values):
        return values.reshape(blocks, span_rows, head_number, values.shape[-1])

    def recur_advance(carried, inputs):
        current_states, running = carried
        query_block, share_block, value_block, decay_blk = inputs
        within_block = jnp.cumsum(decay_blk, axis=0)
        differ = within_block[:, None] - within_block[None, :]
        fading = jnp.exp(jnp.where(lower_tri[:, :, None, None], differ, -jnp.inf))
        scores = jnp.einsum(
            "thk,tshk,shk->tsh", query_block, fading, share_block, precision=HIGHEST_ACCURACY
        )
        inner_part = jnp.einsum("tsh,shv->thv", scores, value_block, precision=HIGHEST_ACCURACY)
        carried_piece = jnp.einsum(
            "zbf,bfw->zbw",
            query_block * jnp.exp(within_block),
            current_states,
            precision=HIGHEST_ACCURACY,
        )
        closing_state = within_block[-1]
        current_states = jnp.exp(closing_state)[:, :, None] * current_states + jnp.einsum(
            "tfo,tfw->fow",
            share_block * jnp.exp(closing_state[None] - within_block),
            value_block,
            precision=HIGHEST_ACCURACY,
        )
        visible_query = query_block * jnp.exp(running[None] + within_block)
        return (
            (current_states, running + closing_state),
            (inner_part + carried_piece, visible_query),
        )

    zeros_run = jnp.zeros((head_number, keydim), jnp.float32)
    (states, running), (outputs, visible_query) = lax.scan(
        recur_advance,
        (states, zeros_run),
        (
            to_blocks(rec_query),
            to_blocks(forget_fraction),
            to_blocks(rec_value),
            to_blocks(decay_logarithm),
        ),
    )
    return (
        outputs.reshape(length, head_number, -1),
        states,
        running,
        visible_query.reshape(length, head_number, keydim),
    )


def attend(
    normalized_input,
    query_weight,
    key_weight,
    value_weight,
    query_norm_gain,
    key_norm_gain,
    cumulative_gate,
    attention_norm_gain,
):
    token_rows = normalized_input.shape[0]
    att_local = query_weight.shape[1] // HEAD_DIM
    sp_index = lax.axis_index("sp")
    queries = rms_rows(
        project(normalized_input, query_weight).reshape(token_rows, att_local, HEAD_DIM),
        query_norm_gain,
    )
    queries = queries.astype(jnp.bfloat16)
    keys = rms_rows(
        project(normalized_input, key_weight).reshape(token_rows, att_local, HEAD_DIM),
        key_norm_gain,
    )
    keys = keys.astype(jnp.bfloat16).reshape(token_rows, att_local * HEAD_DIM)
    values = project(normalized_input, value_weight).astype(jnp.bfloat16)
    all_cum = lax.all_gather(cumulative_gate, "sp", axis=0, tiled=True)
    query_pos = sp_index * token_rows + jnp.arange(token_rows, dtype=jnp.int32)
    query_cum = cumulative_gate.T
    score_scale = HEAD_DIM ** (-0.5)

    def absorb(carried, key_blk, value_block, offset):
        row_top, totals, sums = carried
        width = key_blk.shape[0]
        key_heads = key_blk.reshape(width, att_local, HEAD_DIM)
        value_heads = value_block.reshape(width, att_local, HEAD_DIM)
        key_cum = lax.dynamic_slice_in_dim(all_cum, offset, width, 0).T
        scores = (
            jnp.einsum("qhd,khd->hqk", queries, key_heads, preferred_element_type=jnp.float32)
            * score_scale
        )
        scores = scores + query_cum[:, :, None] - key_cum[:, None, :]
        key_pos = offset + jnp.arange(width, dtype=jnp.int32)
        causal = key_pos[None, :] <= query_pos[:, None]
        scores = jnp.where(causal[None], scores, -jnp.inf)
        new_top = jnp.maximum(row_top, jnp.max(scores, axis=-1))
        anchor = jnp.where(jnp.isfinite(new_top), new_top, 0.0)
        weights = jnp.exp(scores - anchor[:, :, None])
        fading = jnp.exp(row_top - anchor)
        totals = totals * fading + jnp.sum(weights, axis=-1)
        sums = sums * fading[:, :, None] + jnp.einsum(
            "hqk,khd->hqd",
            weights.astype(jnp.bfloat16),
            value_heads,
            preferred_element_type=jnp.float32,
        )
        return (new_top, totals, sums)

    start_carry = (
        jnp.full((att_local, token_rows), -jnp.inf, jnp.float32),
        jnp.zeros((att_local, token_rows), jnp.float32),
        jnp.zeros((att_local, token_rows, HEAD_DIM), jnp.float32),
    )
    carried = start_carry
    key_rows = lax.all_gather(keys, "sp", axis=0, tiled=True)
    value_rows = lax.all_gather(values, "sp", axis=0, tiled=True)
    length = key_rows.shape[0]
    width = math.gcd(length, 512)

    def fold_advance(inner_carry, block_index):
        begin = block_index * width
        key_blk = lax.dynamic_slice_in_dim(key_rows, begin, width, 0)
        value_block = lax.dynamic_slice_in_dim(value_rows, begin, width, 0)
        return (absorb(inner_carry, key_blk, value_block, begin), None)

    carried, ignored = lax.scan(fold_advance, carried, jnp.arange(length // width, dtype=jnp.int32))
    row_top, totals, sums = carried
    attention = (sums / totals[:, :, None]).transpose(1, 0, 2)
    attn_out = rms_rows(attention, attention_norm_gain.reshape(att_local, HEAD_DIM)).astype(
        jnp.bfloat16
    )
    log_sum = (row_top + jnp.log(totals)).T
    return (attn_out.reshape(token_rows, att_local * HEAD_DIM), log_sum)


def recurrence_result(
    normalized_input,
    recurrence_query_weight,
    forget_weight,
    recurrence_value_weight,
    output_gate_weight,
    gate_lower_slack,
    extra_log_decay,
    recurrence_norm_gain,
):
    token_rows = normalized_input.shape[0]
    recurrence_local = recurrence_query_weight.shape[1] // STATE_ROWS
    rec_query = jax.nn.silu(project(normalized_input, recurrence_query_weight)).reshape(
        token_rows, recurrence_local, STATE_ROWS
    )
    forget_fraction = gate_lower_slack * jax.nn.sigmoid(-project(normalized_input, forget_weight))
    decay_logarithm = (
        jnp.log1p(-forget_fraction).reshape(token_rows, recurrence_local, STATE_ROWS)
        + extra_log_decay[:, :, None]
    )
    rec_value = lax.optimization_barrier(
        project(normalized_input, recurrence_value_weight).astype(jnp.bfloat16)
    ).astype(jnp.float32)
    rec_value = rec_value.reshape(token_rows, recurrence_local, VAL_DIM)
    start_states = jnp.zeros((recurrence_local, STATE_ROWS, VAL_DIM), jnp.float32)
    local_output, final_states, run_total, visible_query = recur_blocks(
        rec_query,
        forget_fraction.reshape(token_rows, recurrence_local, STATE_ROWS),
        rec_value,
        decay_logarithm,
        start_states,
    )

    def chain(earlier, later):
        return (earlier[0] + later[0], jnp.exp(later[0])[:, :, None] * earlier[1] + later[1])

    identity = (jnp.zeros_like(run_total), jnp.zeros_like(final_states))
    incoming_state = entering((run_total, final_states), "sp", chain, identity)[1]
    recurrent_output = local_output + jnp.einsum(
        "zbf,bfw->zbw", visible_query, incoming_state, precision=HIGHEST_ACCURACY
    )
    out_gate = jax.nn.silu(project(normalized_input, output_gate_weight)).reshape(
        token_rows, recurrence_local, VAL_DIM
    )
    rec_out = (
        rms_rows(recurrent_output, recurrence_norm_gain.reshape(recurrence_local, VAL_DIM))
        * out_gate
    )
    return rec_out.astype(jnp.bfloat16).reshape(token_rows, recurrence_local * VAL_DIM)


def body(
    layer_input_rows,
    input_norm_gain,
    query_weight,
    key_weight,
    value_weight,
    query_norm_gain,
    key_norm_gain,
    cumulative_gate,
    attention_norm_gain,
    recurrence_query_weight,
    forget_weight,
    recurrence_value_weight,
    output_gate_weight,
    gate_lower_slack,
    extra_log_decay,
    recurrence_norm_gain,
    attention_output_weight,
    recurrence_output_weight,
):
    normalized_input = rms_rows(layer_input_rows.astype(jnp.float32), input_norm_gain).astype(
        jnp.bfloat16
    )
    attn_out, log_sum = attend(
        normalized_input,
        query_weight,
        key_weight,
        value_weight,
        query_norm_gain,
        key_norm_gain,
        cumulative_gate,
        attention_norm_gain,
    )
    rec_out = recurrence_result(
        normalized_input,
        recurrence_query_weight,
        forget_weight,
        recurrence_value_weight,
        output_gate_weight,
        gate_lower_slack,
        extra_log_decay,
        recurrence_norm_gain,
    )
    summed = jnp.dot(attn_out, attention_output_weight, preferred_element_type=jnp.float32)
    mixed_rows = lax.psum_scatter(
        (
            summed + jnp.dot(rec_out, recurrence_output_weight, preferred_element_type=jnp.float32)
        ).astype(jnp.bfloat16),
        "tp",
        scatter_dimension=0,
        tiled=True,
    )
    return (mixed_rows, log_sum)


def solution(mesh):
    return jax.shard_map(
        body,
        mesh=mesh,
        in_specs=(
            P("sp", None),
            P(),
            P(None, "tp"),
            P(None, "tp"),
            P(None, "tp"),
            P(),
            P(),
            P("sp", "tp"),
            P("tp"),
            P(None, "tp"),
            P(None, "tp"),
            P(None, "tp"),
            P(None, "tp"),
            P("tp"),
            P("sp", "tp"),
            P("tp"),
            P("tp", None),
            P("tp", None),
        ),
        out_specs=(P(("sp", "tp"), None), P("sp", "tp")),
        check_vma=False,
    )
```

profile of v0, /device:TPU:29, one launch (start us, length us, event | category | flops | bytes accessed | tf_op | source)
XLA Modules:
  0.0 252.8 jit_solution(15535945552555101778)
XLA Ops:
  8.9 2.2 bitcast_reduce_fusion
  13.5 1.8 negate_log-plus-one_fusion
  16.4 1.7 divide_multiply_fusion.1
  18.3 1.7 convolution_convert_fusion
  21.5 59.6 %while.47 = (s32[]{:T(128)}, f32[2,128,128]{2,1,0:T(8,128)S(1)}, f32[2,128]{1,0:T(2,128)S(1)}, f32[4,64,2,128]{3,1,0,2:T(8,128)}, f32[4,64,2,128]{3,2,1,0:T(2,12...) while((s32[]{:T(128)}, f32[2,128,128]{2,1,0:T(8,128)S(1)}, ...), condition=%wide.region_10.11_spmd.clone, body=%wide.region_8.10_spmd.clone.sunk | while | flops 79909376 | bytes 10439809 | solution.py:89
  22.4 5.9 %multiply_bitcast_fusion.2 = f32[64,2,128,64]{2,1,0,3:T(2,128)S(1)} fusion(pred[64,64]{1,0:T(8,128)(4,1)S(1)} %iota_compare_fusion.2, f32[64,2,128]{2,1,0:T(2,128)S(1)} %get-tuple-element.615, f32[64,2,128]{2,1,0:T(2,128)S(1)} %fusion.113), kind=kLoop, calls=%fused_computation.22.clone.1 | loop fusion | flops 3145728 | bytes 4329472 | tf_op jit(solution)/shard_map/while/body/eval_jaxpr/thk,tshk,shk->tsh/dot_general | solution.py:65
  28.3 6.6 %fusion.116 = f32[64,2,1,64]{3,2,1,0:T(1,128)S(1)} fusion(f32[64,2,128,1]{2,3,1,0:T(1,128)S(1)} %bitcast.162, f32[64,2,128,64]{2,1,0,3:T(2,128)S(1)} %multiply_bitcast_fusion.2), kind=kOutput, calls=%fused_computation.20.clone.1 | convolution fusion | flops 12582912 | bytes 4292608 | tf_op jit(solution)/shard_map/while/body/eval_jaxpr/thk,tshk,shk->tsh/dot_general | solution.py:65
  37.3 5.9 %multiply_bitcast_fusion.2 = f32[64,2,128,64]{2,1,0,3:T(2,128)S(1)} fusion(pred[64,64]{1,0:T(8,128)(4,1)S(1)} %iota_compare_fusion.2, f32[64,2,128]{2,1,0:T(2,128)S(1)} %get-tuple-element.615, f32[64,2,128]{2,1,0:T(2,128)S(1)} %fusion.113), kind=kLoop, calls=%fused_computation.22.clone.1 | loop fusion | flops 3145728 | bytes 4329472 | tf_op jit(solution)/shard_map/while/body/eval_jaxpr/thk,tshk,shk->tsh/dot_general | solution.py:65
  43.2 6.6 %fusion.116 = f32[64,2,1,64]{3,2,1,0:T(1,128)S(1)} fusion(f32[64,2,128,1]{2,3,1,0:T(1,128)S(1)} %bitcast.162, f32[64,2,128,64]{2,1,0,3:T(2,128)S(1)} %multiply_bitcast_fusion.2), kind=kOutput, calls=%fused_computation.20.clone.1 | convolution fusion | flops 12582912 | bytes 4292608 | tf_op jit(solution)/shard_map/while/body/eval_jaxpr/thk,tshk,shk->tsh/dot_general | solution.py:65
  52.2 5.9 %multiply_bitcast_fusion.2 = f32[64,2,128,64]{2,1,0,3:T(2,128)S(1)} fusion(pred[64,64]{1,0:T(8,128)(4,1)S(1)} %iota_compare_fusion.2, f32[64,2,128]{2,1,0:T(2,128)S(1)} %get-tuple-element.615, f32[64,2,128]{2,1,0:T(2,128)S(1)} %fusion.113), kind=kLoop, calls=%fused_computation.22.clone.1 | loop fusion | flops 3145728 | bytes 4329472 | tf_op jit(solution)/shard_map/while/body/eval_jaxpr/thk,tshk,shk->tsh/dot_general | solution.py:65
  58.1 6.6 %fusion.116 = f32[64,2,1,64]{3,2,1,0:T(1,128)S(1)} fusion(f32[64,2,128,1]{2,3,1,0:T(1,128)S(1)} %bitcast.162, f32[64,2,128,64]{2,1,0,3:T(2,128)S(1)} %multiply_bitcast_fusion.2), kind=kOutput, calls=%fused_computation.20.clone.1 | convolution fusion | flops 12582912 | bytes 4292608 | tf_op jit(solution)/shard_map/while/body/eval_jaxpr/thk,tshk,shk->tsh/dot_general | solution.py:65
  67.1 5.9 %multiply_bitcast_fusion.2 = f32[64,2,128,64]{2,1,0,3:T(2,128)S(1)} fusion(pred[64,64]{1,0:T(8,128)(4,1)S(1)} %iota_compare_fusion.2, f32[64,2,128]{2,1,0:T(2,128)S(1)} %get-tuple-element.615, f32[64,2,128]{2,1,0:T(2,128)S(1)} %fusion.113), kind=kLoop, calls=%fused_computation.22.clone.1 | loop fusion | flops 3145728 | bytes 4329472 | tf_op jit(solution)/shard_map/while/body/eval_jaxpr/thk,tshk,shk->tsh/dot_general | solution.py:65
  73.0 6.6 %fusion.116 = f32[64,2,1,64]{3,2,1,0:T(1,128)S(1)} fusion(f32[64,2,128,1]{2,3,1,0:T(1,128)S(1)} %bitcast.162, f32[64,2,128,64]{2,1,0,3:T(2,128)S(1)} %multiply_bitcast_fusion.2), kind=kOutput, calls=%fused_computation.20.clone.1 | convolution fusion | flops 12582912 | bytes 4292608 | tf_op jit(solution)/shard_map/while/body/eval_jaxpr/thk,tshk,shk->tsh/dot_general | solution.py:65
  81.2 26.0 %all-gather.1 = bf16[16,128,128]{2,1,0:T(8,128)(2,1)S(1)} all-gather(bf16[2,128,128]{2,1,0:T(8,128)(2,1)S(1)} %convert_element_type.68), channel_id=3, replica_groups=mesh['sp'=8,'tp'=4] {'sp'}, dimensions={0}, use_global_device_ids=true | all-gather | bytes 589824 | tf_op jit(solution)/shard_map/all_gather | solution.py:21
  107.2 12.8 %all-gather.2 = bf16[8,2,128]{2,1,0:T(2,128)(2,1)S(1)} all-gather(bf16[1,2,128]{2,1,0:T(2,128)(2,1)S(1)} %convert_bitcast_fusion), channel_id=2, replica_groups=mesh['sp'=8,'tp'=4] {'sp'}, dimensions={0}, use_global_device_ids=true | all-gather | bytes 4608 | tf_op jit(solution)/shard_map/all_gather | solution.py:21
  121.5 1.8 divide_multiply_fusion
  124.1 26.4 %all_gather.22 = f32[2048,4]{0,1:T(4,128)} all-gather(f32[256,4]{0,1:T(4,128)} %param.31), channel_id=1, replica_groups=mesh['sp'=8,'tp'=4] {'sp'}, dimensions={0}, use_global_device_ids=true | all-gather | bytes 36864 | tf_op jit(solution)/shard_map/all_gather | solution.py:131
  151.0 1.9 multiply_reduce_fusion.1
  154.4 46.3 %while.46 = (s32[]{:T(128)}, f32[4,256]{1,0:T(4,128)S(1)}, f32[4,256]{1,0:T(4,128)}, f32[4,256,64]{1,2,0:T(8,128)}, s32[4]{0:T(128)}, /*index=5*/bf16[2048,256]{...) while((s32[]{:T(128)}, f32[4,256]{1,0:T(4,128)S(1)}, ...), condition=%wide.region_6.7_spmd.clone, body=%wide.region_3.6_spmd.clone.sunk | while | flops 139273984 | bytes 9410791 | solution.py:180
  171.8 1.7 constant_dynamic-slice_fusion.8
  174.6 2.1 convolution_add_fusion.5
  186.6 2.1 convolution_add_fusion.5
  198.6 2.1 convolution_add_fusion.5
  206.1 40.2 %reduce-scatter.2.cloned.1.call-done = bf16[64,2048]{1,0:T(8,128)(2,1)} async-done(((bf16[256,2048]{1,0:T(8,128)(2,1)}), bf16[64,2048]{1,0:T(8,128)(2,1)}) %reduce-scatter.2.cloned.1.call-update) | async-done | bytes 262160 | tf_op jit(solution)/shard_map/reduce_scatter | solution.py:285
  (179 shorter events, 62.1 us)
Async XLA Ops:
  7.2 195.7 %copy-start = (bf16[256,2048]{1,0:T(8,128)(2,1)S(1)}, bf16[256,2048]{1,0:T(8,128)(2,1)}, u32[]{:S(2)}) copy-start(bf16[256,2048]{1,0:T(8,128)(2,1)} %param.40) | copy-start | bytes 3145732
  7.2 5.0 %copy-start.1 = (bf16[256,2048]{1,0:T(8,128)(2,1)S(1)}, bf16[256,2048]{1,0:T(8,128)(2,1)}, u32[]{:S(2)}) copy-start(bf16[256,2048]{1,0:T(8,128)(2,1)} %param.24) | copy-start | bytes 3145732
  7.2 5.0 %copy-start.11 = (f32[2048]{0:T(1024)S(1)}, f32[2048]{0:T(1024)}, u32[]{:S(2)}) copy-start(f32[2048]{0:T(1024)} %param.25) | copy-start | bytes 24580
  7.2 4.0 %copy-start.9 = (f32[64]{0:T(128)S(1)}, f32[64]{0:T(128)}, u32[]{:S(2)}) copy-start(f32[64]{0:T(128)} %param.30) | copy-start | bytes 772
  7.2 4.9 %copy-start.10 = (bf16[2048,256]{1,0:T(8,128)(2,1)S(1)}, bf16[2048,256]{1,0:T(8,128)(2,1)}, u32[]{:S(2)}) copy-start(bf16[2048,256]{1,0:T(8,128)(2,1)} %param.28) | copy-start | bytes 3145732
  7.2 146.5 %all-gather.6.cloned.1.call-start = ((), (), s32[]{:S(2)}) async-start(), calls=%async_computation.1 | async-start | bytes 1179648 | tf_op jit(solution)/shard_map/all_gather | solution.py:169
  11.2 2.3 copy-start.13
  12.1 141.7 %all-gather.8.cloned.1.call-start = ((), (), s32[]{:S(2)}) async-start(), calls=%async_computation.2 | async-start | bytes 1179648 | tf_op jit(solution)/shard_map/all_gather | solution.py:170
  13.3 232.9 %reduce-scatter.2.cloned.1.call-start = ((), (), s32[]{:S(2)}) async-start(), calls=%async_computation.3 | async-start | bytes 1310720 | tf_op jit(solution)/shard_map/reduce_scatter | solution.py:285
  13.4 2.7 %copy-start.5 = (f32[256,2]{0,1:T(2,128)S(1)}, f32[256,2]{0,1:T(2,128)}, u32[]{:S(2)}) copy-start(f32[256,2]{0,1:T(2,128)} %param.38) | copy-start | bytes 6148
  81.1 40.2 %copy-start.4 = (f32[4,64,2,128]{3,1,0,2:T(8,128)S(1)}, f32[4,64,2,128]{3,1,0,2:T(8,128)}, u32[]{:S(2)}) copy-start(f32[4,64,2,128]{3,1,0,2:T(8,128)} %get-tuple-element.212) | copy-start | bytes 786436
  81.1 40.4 %copy-start.12 = (f32[2048]{0:T(1024)S(1)}, f32[2048]{0:T(1024)}, u32[]{:S(2)}) copy-start(f32[2048]{0:T(1024)} %param.25) | copy-start | bytes 24580
  121.5 2.0 copy-start.7
  121.5 29.0 %copy-start.3 = (f32[4,64,2,128]{3,2,1,0:T(2,128)S(1)}, f32[4,64,2,128]{3,2,1,0:T(2,128)}, u32[]{:S(2)}) copy-start(f32[4,64,2,128]{3,2,1,0:T(2,128)} %get-tuple-element.216) | copy-start | bytes 786436
  123.4 29.4 %copy-start.8 = (f32[64]{0:T(128)S(1)}, f32[64]{0:T(128)}, u32[]{:S(2)}) copy-start(f32[64]{0:T(128)} %param.29) | copy-start | bytes 772
  150.5 3.1 %copy-start.6 = (f32[256]{0:T(256)S(1)}, f32[256]{0:T(256)}, u32[]{:S(2)}) copy-start(f32[256]{0:T(256)} %param.39) | copy-start | bytes 3076
  200.7 2.6 %copy-start.2 = (bf16[256,2048]{1,0:T(8,128)(2,1)S(1)}, bf16[256,2048]{1,0:T(8,128)(2,1)}, u32[]{:S(2)}) copy-start(bf16[256,2048]{1,0:T(8,128)(2,1)} %param.41) | copy-start | bytes 3145732
Sparse Core Ops, SparseCore 0:
  12.2 36.6 all-gather.5
  51.0 38.9 all-gather.7
  204.9 41.2 reduce-scatter.1
where the time goes:
time: 256 us; the launch traced here: 253 us
  blocking collectives  65.1 us (25%)
  matrix products  60.9 us (24%)
  other arithmetic  42.7 us (17%)
  waiting for transfers between devices  40.3 us (16%)
  local copies, waits for them, and re-layouts  26 us (10%)
  between operations  14.2 us (6%)
  loops' own time  3.43 us (1%)
    reduce_scatter x1, waiting for transfers between devices, body(): lax.psum_scatter((summed + jnp.dot(rec_out, recurrence_output_weight, pre...  40.2 us
    all_gather x2, blocking collectives, entering(): lax.all_gather(part.astype(kind), axis)  38.8 us
    all_gather x1, blocking collectives, attend(): all_cum = lax.all_gather(cumulative_gate, 'sp', axis=0, tiled=True)  26.4 us
    dot_general x4, matrix products, recur_advance(): jnp.einsum('thk,tshk,shk->tsh', query_block, fading, share_block, precisi...  26.3 us
    dot_general x4, other arithmetic, recur_advance(): jnp.einsum('thk,tshk,shk->tsh', query_block, fading, share_block, precisi...  23.6 us
    dot_general x7, matrix products, project(): return jnp.dot(normalized_input, weight, preferred_element_type=jnp.float32)  12.3 us
    dynamic_slice x8, local copies, waits for them, and re-layouts, fold_advance(): value_block = lax.dynamic_slice_in_dim(value_rows, begin, width, 0)  11 us
    dot_general x4, matrix products, absorb(): jnp.einsum('hqk,khd->hqd', weights.astype(jnp.bfloat16), value_heads, pre...  7.53 us
  transfers between devices with their start and end apart: 3, of which 1 were waited for; matrix products, arithmetic and copies ran while one was open for 30% of the time, Pallas kernels for 0%

commit v1 on v0

v1 whole, which is shorter than its diff:
```python
import functools
import math

import jax
import jax.numpy as jnp
from jax import lax
from jax.experimental import pallas as pl
from jax.experimental.pallas import tpu as pltpu
from jax.sharding import PartitionSpec as P

HEAD_DIM = 64
STATE_ROWS = 128
LANES = 128
EPSILON = 1e-06
HIGHEST = lax.Precision.HIGHEST
MESH = pl.DeviceIdType.MESH
F32 = jnp.float32
BF16 = jnp.bfloat16


def dot(a, b):
    return jnp.dot(a, b, preferred_element_type=F32)


def dot_exact(a, b):
    return jnp.dot(a, b, preferred_element_type=F32, precision=HIGHEST)


def dot_nt(a, b, precision=None):
    return lax.dot_general(
        a, b, (((1,), (1,)), ((), ())), preferred_element_type=F32, precision=precision
    )


def iota(shape, axis):
    return lax.broadcasted_iota(jnp.int32, shape, axis)


def grid_of(count):
    columns = max(c for c in range(1, math.isqrt(count) + 1) if count % c == 0)
    return count // columns, columns


def kernel(
    sizes,
    x_hbm, wk_hbm, wv_hbm, wf_hbm, wrv_hbm, wrq_hbm, wq_hbm, wog_hbm, wao_hbm, wro_hbm,
    in_gain, q_gain, k_gain, gate_t, a_gain, slack, extra_t, r_gain,
    mixed_ref, logsum_ref,
    x_v, wk_v, wv_v, wf_v, wrv_v, wrq_v, wq_v, wog_v, wao_v, wro_v,
    xn, kv, gates, q_t, m_s, l_s, acc, attn_t,
    inner, vq, og, ext, st, chain_in, chain_out, incoming, part, mine, send2, recv1, recv2,
    load_sem, col_send, row_send, recv_sem, st_send, st_recv, chain_send, chain_recv,
    s1_send, s1_recv, s2_send, s2_recv,
):
    nz, ny, ntp = sizes
    rows, width = x_v.shape
    cols = wk_v.shape[1]
    heads = cols // HEAD_DIM
    pairs = cols // LANES
    rec_heads = cols // STATE_ROWS
    chips = ntp // 2
    rb = rows // ntp
    pieces = rows // LANES
    stride = rows + pieces * LANES

    sp, tp = lax.axis_index("sp"), lax.axis_index("tp")
    z, y = sp // ny, sp % ny
    chip, core = tp // 2, tp % 2
    partner = chip * 2 + (1 - core)

    loads = []
    for i, (src, dst) in enumerate((
        (x_hbm, x_v), (wk_hbm, wk_v), (wv_hbm, wv_v), (wf_hbm, wf_v), (wrv_hbm, wrv_v),
        (wrq_hbm, wrq_v), (wq_hbm, wq_v), (wog_hbm, wog_v), (wao_hbm, wao_v), (wro_hbm, wro_v),
    )):
        loads.append(pltpu.make_async_copy(src, dst, load_sem.at[i]))
        loads[-1].start()

    barrier = pltpu.get_barrier_semaphore()

    def greet(where):
        pl.semaphore_signal(barrier, inc=1, device_id=where, device_id_type=MESH)

    @pl.when(z > 0)
    def _():
        greet((sp - ny, tp))

    @pl.when(z < nz - 1)
    def _():
        greet((sp + ny, tp))

    for k in range(1, ny):
        greet((z * ny + (y + k) % ny, tp))
    greet((sp, partner))
    for k in range(1, chips):
        greet((sp, ((chip + k) % chips) * 2 + core))

    loads[0].wait()
    xf = x_v[...].astype(F32)
    scale = lax.rsqrt(jnp.mean(xf * xf, axis=-1, keepdims=True) + EPSILON)
    xn[...] = (xf * scale * in_gain[...]).astype(BF16)

    block_ones = jnp.where(
        iota((cols, cols), 0) // HEAD_DIM == iota((cols, cols), 1) // HEAD_DIM, 1.0 / HEAD_DIM, 0.0
    ).astype(F32)
    repeat = (iota((HEAD_DIM, cols), 1) % HEAD_DIM == iota((HEAD_DIM, cols), 0)).astype(F32)

    def head_norm(v, gain_ref):
        mean = dot_exact(v * v, block_ones)
        gain = dot_exact(jnp.broadcast_to(gain_ref[...], (8, HEAD_DIM)), repeat)[0:1]
        return v * lax.rsqrt(mean + EPSILON) * gain

    loads[1].wait()
    keys = head_norm(dot(xn[...], wk_v[...]), k_gain).astype(BF16)
    loads[2].wait()
    values_t = dot(xn[...], wv_v[...]).T.astype(BF16)
    for p in range(pairs):
        lanes = slice(p * LANES, (p + 1) * LANES)
        kv[sp, p * stride : p * stride + rows, :] = keys[:, lanes]
        for i in range(pieces):
            at = p * stride + rows + i * LANES
            kv[sp, at : at + LANES, :] = values_t[lanes, i * LANES : (i + 1) * LANES]
    gates[sp] = jnp.zeros((8, rows), F32)
    gates[sp, 0:heads, :] = gate_t[...]

    def kv_copies(slot, send_sems, where):
        return [
            pltpu.make_async_remote_copy(
                src_ref=buf.at[slot], dst_ref=buf.at[slot], send_sem=send_sems.at[i],
                recv_sem=recv_sem.at[slot, i], device_id=where, device_id_type=MESH,
            )
            for i, buf in enumerate((gates, kv))
        ]

    def up_copies(source_z):
        return kv_copies(source_z * ny + y, col_send.at[source_z], (sp + ny, tp))

    def side_copies(source_z, k):
        return kv_copies(
            source_z * ny + y, row_send.at[source_z, k], (z * ny + (y + k) % ny, tp)
        )

    def wait_block(slot):
        for copy in kv_copies(slot, col_send.at[0], (sp, partner)):
            copy.wait_recv()

    greeted = (ny - 1) + chips + (z > 0).astype(jnp.int32) + (z < nz - 1).astype(jnp.int32)
    pl.semaphore_wait(barrier, greeted)

    @pl.when(z < nz - 1)
    def _():
        for copy in up_copies(z):
            copy.start()

    for k in range(1, ny):
        @pl.when(y + k < ny)
        def _():
            for copy in side_copies(z, k):
                copy.start()

    tri = (iota((rows, rows), 0) >= iota((rows, rows), 1)).astype(F32)
    loads[3].wait()
    share = slack[...] / (1.0 + jnp.exp(dot(xn[...], wf_v[...])))
    run = dot_exact(tri, jnp.log1p(-share))
    ext[...] = jnp.zeros_like(ext)
    ext[0:rec_heads, :] = extra_t[...]
    ext_row = dot_nt(ext[...], tri, HIGHEST)
    ext_col = dot_nt(tri, ext[...], HIGHEST)
    loads[4].wait()
    rec_value = dot(xn[...], wrv_v[...])
    loads[5].wait()
    rec_query = dot(xn[...], wrq_v[...])
    rec_query = rec_query / (1.0 + jnp.exp(-rec_query))
    grown = rec_query * jnp.exp(run)
    last = run[rows - 1 : rows]
    st_rows = STATE_ROWS + 16
    for j in range(rec_heads):
        lanes = slice(j * STATE_ROWS, (j + 1) * STATE_ROWS)
        e_col = ext_col[:, j : j + 1]
        e_row = ext_row[j : j + 1, :]
        e_last = e_row[:, rows - 1 : rows]
        value = rec_value[:, lanes].astype(BF16)
        left = share[:, lanes] * jnp.exp(last[:, lanes] - run[:, lanes] + (e_last - e_col))
        st[y, j * st_rows : j * st_rows + STATE_ROWS, :] = dot(
            rec_value[:, lanes].T.astype(BF16), left.astype(BF16)
        ).astype(BF16)
        st[y, j * st_rows + STATE_ROWS : (j + 1) * st_rows, :] = jnp.broadcast_to(
            jnp.exp(last[:, lanes] + e_last), (16, STATE_ROWS)
        ).astype(BF16)
        scores = dot_nt(
            grown[:, lanes].astype(BF16), (share[:, lanes] * jnp.exp(-run[:, lanes])).astype(BF16)
        )
        fading = jnp.exp(jnp.where(tri > 0.5, e_col - e_row, -jnp.inf))
        scores = jnp.where(tri > 0.5, scores * fading, 0.0)
        inner[:, lanes] = dot(scores.astype(BF16), value)
        vq[:, lanes] = (grown[:, lanes] * jnp.exp(e_col)).astype(BF16)

    def st_copy(k):
        return pltpu.make_async_remote_copy(
            src_ref=st.at[y], dst_ref=st.at[y], send_sem=st_send.at[k], recv_sem=st_recv.at[y],
            device_id=(z * ny + (y + k) % ny, tp), device_id_type=MESH,
        )

    for k in range(1, ny):
        st_copy(k).start()

    loads[6].wait()
    queries_t = (head_norm(dot(xn[...], wq_v[...]), q_gain).astype(BF16).astype(F32)).T
    half_of = iota((LANES, rows), 0) // HEAD_DIM
    for h in range(heads):
        pair = queries_t[(h // 2) * LANES : (h // 2 + 1) * LANES, :] * HEAD_DIM ** (-0.5)
        q_t[h] = jnp.where(half_of == h % 2, pair, 0.0).astype(BF16)

    def attend(slot, own):
        gate = gates[slot].T
        for h in range(heads):
            base = (h // 2) * stride
            s = dot(kv[slot, base : base + rows, :], q_t[h]) - gate[:, h : h + 1]
            if own:
                s = jnp.where(iota((rows, rows), 0) <= iota((rows, rows), 1), s, -jnp.inf)
                top = jnp.max(s, axis=0, keepdims=True)
            else:
                top = jnp.maximum(m_s[h], jnp.max(s, axis=0, keepdims=True))
            weights = jnp.exp(s - top)
            total = jnp.sum(weights, axis=0, keepdims=True)
            at = base + rows + (h % 2) * HEAD_DIM
            v_t = jnp.concatenate(
                [kv[slot, at + i * LANES : at + i * LANES + HEAD_DIM, :] for i in range(pieces)],
                axis=1,
            )
            summed = dot(v_t, weights.astype(BF16))
            if own:
                l_s[h] = total
                acc[h] = summed
            else:
                fade = jnp.exp(m_s[h] - top)
                l_s[h] = l_s[h] * fade + total
                acc[h] = acc[h] * fade + summed
            m_s[h] = top

    attend(sp, True)

    loads[7].wait()
    gate_out = dot(xn[...], wog_v[...])
    og[...] = gate_out / (1.0 + jnp.exp(-gate_out))

    for k in range(1, ny):
        other = (y + k) % ny
        pltpu.make_async_remote_copy(
            src_ref=st.at[other], dst_ref=st.at[other], send_sem=st_send.at[0],
            recv_sem=st_recv.at[other], device_id=(sp, partner), device_id_type=MESH,
        ).wait_recv()

    chain_copy = pltpu.make_async_remote_copy(
        src_ref=chain_out, dst_ref=chain_in, send_sem=chain_send, recv_sem=chain_recv,
        device_id=((sp + ny) % (nz * ny), tp), device_id_type=MESH,
    )

    def advance_chain():
        for j in range(rec_heads):
            rows_at = slice(j * STATE_ROWS, (j + 1) * STATE_ROWS)
            state = chain_in[rows_at, :].astype(F32)
            for k in range(ny):
                @pl.when(y == k)
                def _():
                    incoming[rows_at, :] = state.astype(BF16)

                base = j * st_rows
                decay = st[k, base + STATE_ROWS : base + st_rows, :].astype(F32)[0:1]
                state = state * decay + st[k, base : base + STATE_ROWS, :].astype(F32)
            chain_out[rows_at, :] = state.astype(BF16)

        @pl.when(z < nz - 1)
        def _():
            chain_copy.start()

    @pl.when(z == 0)
    def _():
        chain_in[...] = jnp.zeros_like(chain_in)
        advance_chain()

    for k in range(1, ny):
        @pl.when(y - k >= 0)
        def _():
            wait_block(sp - k)
            attend(sp - k, False)

    def step(d, carry):
        source = z - d
        wait_block(source * ny + y)

        @pl.when(z < nz - 1)
        def _():
            for copy in up_copies(source):
                copy.start()

        for k in range(1, ny):
            for copy in side_copies(source, k):
                copy.start()

        attend(source * ny + y, False)

        @pl.when(d == jnp.maximum(z - 1, 1))
        def _():
            chain_copy.wait_recv()
            advance_chain()

        for k in range(1, ny):
            slot = source * ny + (y + k) % ny
            wait_block(slot)
            attend(slot, False)
        return carry

    lax.fori_loop(1, z + 1, step, 0)

    for h in range(heads):
        mixed = acc[h] / l_s[h]
        mean = jnp.mean(mixed * mixed, axis=0, keepdims=True)
        attn_t[h * HEAD_DIM : (h + 1) * HEAD_DIM, :] = mixed * lax.rsqrt(mean + EPSILON)
        logsum_ref[h : h + 1, :] = m_s[h] + jnp.log(l_s[h]) + gate_t[h : h + 1, :]
    attn_out = (attn_t[...].T * a_gain[...]).astype(BF16)
    for j in range(rec_heads):
        lanes = slice(j * STATE_ROWS, (j + 1) * STATE_ROWS)
        out = inner[:, lanes] + dot_nt(vq[:, lanes], incoming[lanes, :])
        mean = jnp.mean(out * out, axis=-1, keepdims=True)
        out = out * lax.rsqrt(mean + EPSILON) * r_gain[:, lanes] * og[:, lanes]
        vq[:, lanes] = out.astype(BF16)
    loads[8].wait()
    loads[9].wait()
    part[...] = (dot(attn_out, wao_v[...]) + dot(vq[...], wro_v[...])).astype(BF16)

    def rows_of(which_chip, which_core):
        return pl.ds(pl.multiple_of((which_chip * 2 + which_core) * rb, rb), rb)

    def within(j):
        return pltpu.make_async_remote_copy(
            src_ref=part.at[rows_of(j, 1 - core)], dst_ref=recv1.at[j], send_sem=s1_send.at[j],
            recv_sem=s1_recv.at[j], device_id=(sp, partner), device_id_type=MESH,
        )

    def between(j):
        return pltpu.make_async_remote_copy(
            src_ref=send2.at[j], dst_ref=recv2.at[chip], send_sem=s2_send.at[j],
            recv_sem=s2_recv.at[chip], device_id=(sp, j * 2 + core), device_id_type=MESH,
        )

    order = [(chip + k) % chips for k in range(1, chips)] + [chip]
    for j in order:
        within(j).start()
    for j in order[:-1]:
        within(j).wait_recv()
        send2[j] = (part[rows_of(j, core), :].astype(F32) + recv1[j].astype(F32)).astype(BF16)
        between(j).start()
    within(chip).wait_recv()
    mine[...] = part[rows_of(chip, core), :].astype(F32) + recv1[chip].astype(F32)
    for j in order[:-1]:
        pltpu.make_async_remote_copy(
            src_ref=send2.at[j], dst_ref=recv2.at[j], send_sem=s2_send.at[j],
            recv_sem=s2_recv.at[j], device_id=(sp, partner), device_id_type=MESH,
        ).wait_recv()
        mine[...] += recv2[j].astype(F32)
    mixed_ref[...] = mine[...].astype(BF16)

    for j in order:
        within(j).wait_send()
    for j in order[:-1]:
        between(j).wait_send()
    for k in range(1, ny):
        st_copy(k).wait_send()

        @pl.when(y + k < ny)
        def _():
            for copy in side_copies(z, k):
                copy.wait_send()

    @pl.when(z < nz - 1)
    def _():
        chain_copy.wait_send()
        for copy in up_copies(z):
            copy.wait_send()

    def drain(d, carry):
        source = z - d

        @pl.when(z < nz - 1)
        def _():
            for copy in up_copies(source):
                copy.wait_send()

        for k in range(1, ny):
            for copy in side_copies(source, k):
                copy.wait_send()
        return carry

    lax.fori_loop(1, z + 1, drain, 0)


def body(
    n_sp, n_tp,
    layer_input_rows, input_norm_gain, query_weight, key_weight, value_weight, query_norm_gain,
    key_norm_gain, cumulative_gate, attention_norm_gain, recurrence_query_weight, forget_weight,
    recurrence_value_weight, output_gate_weight, gate_lower_slack, extra_log_decay,
    recurrence_norm_gain, attention_output_weight, recurrence_output_weight,
):
    nz, ny = grid_of(n_sp)
    rows, width = layer_input_rows.shape
    cols = query_weight.shape[1]
    heads, pairs, rec_heads = cols // HEAD_DIM, cols // LANES, cols // STATE_ROWS
    rb, chips = rows // n_tp, n_tp // 2
    weight = pltpu.VMEM((width, cols), BF16)
    out_weight = pltpu.VMEM((cols, width), BF16)
    dma = pltpu.SemaphoreType.DMA
    any_space = pl.BlockSpec(memory_space=pl.ANY)
    vmem = pl.BlockSpec(memory_space=pltpu.VMEM)
    mixed, log_sum = pl.pallas_call(
        functools.partial(kernel, (nz, ny, n_tp)),
        name="mixer",
        out_shape=(
            jax.ShapeDtypeStruct((rb, width), BF16),
            jax.ShapeDtypeStruct((heads, rows), F32),
        ),
        in_specs=[any_space] * 10 + [vmem] * 8,
        out_specs=(vmem, vmem),
        scratch_shapes=[
            pltpu.VMEM((rows, width), BF16),
            *([weight] * 7), out_weight, out_weight,
            pltpu.VMEM((rows, width), BF16),
            pltpu.VMEM((n_sp, pairs * 2 * rows, LANES), BF16),
            pltpu.VMEM((n_sp, 8, rows), F32),
            pltpu.VMEM((heads, LANES, rows), BF16),
            pltpu.VMEM((heads, 1, rows), F32),
            pltpu.VMEM((heads, 1, rows), F32),
            pltpu.VMEM((heads, HEAD_DIM, rows), F32),
            pltpu.VMEM((cols, rows), F32),
            pltpu.VMEM((rows, cols), F32),
            pltpu.VMEM((rows, cols), BF16),
            pltpu.VMEM((rows, cols), F32),
            pltpu.VMEM((8, rows), F32),
            pltpu.VMEM((ny, rec_heads * (STATE_ROWS + 16), STATE_ROWS), BF16),
            pltpu.VMEM((cols, STATE_ROWS), BF16),
            pltpu.VMEM((cols, STATE_ROWS), BF16),
            pltpu.VMEM((cols, STATE_ROWS), BF16),
            pltpu.VMEM((rows, width), BF16),
            pltpu.VMEM((rb, width), F32),
            pltpu.VMEM((chips, rb, width), BF16),
            pltpu.VMEM((chips, rb, width), BF16),
            pltpu.VMEM((chips, rb, width), BF16),
            dma((10,)),
            dma((nz, 2)), dma((nz, ny, 2)), dma((n_sp, 2)),
            dma((ny,)), dma((ny,)), dma, dma,
            dma((chips,)), dma((chips,)), dma((chips,)), dma((chips,)),
        ],
        compiler_params=pltpu.CompilerParams(
            collective_id=0, has_side_effects=True, vmem_limit_bytes=60 * 1024 * 1024
        ),
    )(
        layer_input_rows, key_weight, value_weight, forget_weight, recurrence_value_weight,
        recurrence_query_weight, query_weight, output_gate_weight, attention_output_weight,
        recurrence_output_weight,
        input_norm_gain.reshape(1, -1), query_norm_gain.reshape(1, -1),
        key_norm_gain.reshape(1, -1), cumulative_gate.T, attention_norm_gain.reshape(1, -1),
        gate_lower_slack.reshape(1, -1), extra_log_decay.T, recurrence_norm_gain.reshape(1, -1),
    )
    return mixed, log_sum.T


def solution(mesh):
    return jax.shard_map(
        functools.partial(body, mesh.shape["sp"], mesh.shape["tp"]),
        mesh=mesh,
        in_specs=(
            P("sp", None),
            P(),
            P(None, "tp"),
            P(None, "tp"),
            P(None, "tp"),
            P(),
            P(),
            P("sp", "tp"),
            P("tp"),
            P(None, "tp"),
            P(None, "tp"),
            P(None, "tp"),
            P(None, "tp"),
            P("tp"),
            P("sp", "tp"),
            P("tp"),
            P("tp", None),
            P("tp", None),
        ),
        out_specs=(P(("sp", "tp"), None), P("sp", "tp")),
        check_vma=False,
    )
```

time: 256 us -> 50.6 us (0.20)
  the two profiles are of different devices: /device:TPU:29 before, /device:TPU:25 now
where the time goes in v1:
time: 50.6 us; the launch traced here: 50.5 us
  Pallas kernels  47.5 us (94%)
  local copies, waits for them, and re-layouts  2.27 us (4%)
  between operations  0.65 us (1%)
    pallas_call x1, Pallas kernels, body(): pl.pallas_call(functools.partial(kernel, (nz, ny, n_tp)), name='mixer', o...  47.5 us
    unnamed x4, local copies, waits for them, and re-layouts  2.27 us

profile of v1, /device:TPU:25, one launch (start us, length us, event | category | flops | bytes accessed | tf_op | source)
XLA Modules:
  0.0 50.5 jit_solution(15651650106441310392)
XLA Ops:
  0.6 47.5 %mixer.1 = (bf16[64,2048]{1,0:T(8,128)(2,1)}, f32[4,256]{1,0:T(4,128)}) custom-call(bf16[256,2048]{1,0:T(8,128)(2,1)} %x_hbm.1, bf16[2048,256]{1,0:T(8,128)(2,1)} %wk_hbm.1, bf16[2048,256]{1,0:T(8,128)(2,1)} %wv_hbm.1, bf16[2048,256]{1,0:T(8,128)(2,1)} %wf_hbm.1, bf16[2048,256]{1,0:T(8,128)(2,1)} %wrv_hbm.1, bf16[2048,256]{1,0:T(8,128)(2,1)} %wrq_hbm.1, ...), custom_call_target="tpu_custom_call" | custom-call | tf_op jit(solution)/shard_map/mixer/pallas_call | solution.py:415
  48.2 0.0 copy-start
  48.2 1.7 %copy.22 = bf16[64,2048]{1,0:T(8,128)(2,1)} copy(bf16[64,2048]{1,0:T(8,128)(2,1)} %get-tuple-element.8) | data formatting | bytes 524288
  49.9 0.0 copy-done
  49.9 0.6 %copy.23 = f32[256,4]{0,1:T(4,128)} copy(f32[256,4]{0,1:T(4,128)S(1)} %bitcast.11) | data formatting | bytes 8192
Async XLA Ops:
  48.2 1.7 %copy-start = (f32[4,256]{1,0:T(4,128)S(1)}, f32[4,256]{1,0:T(4,128)}, u32[]{:S(2)}) copy-start(f32[4,256]{1,0:T(4,128)} %get-tuple-element.5) | copy-start | bytes 12292

commit v2 on v1

--- a/solution.py
+++ b/solution.py
@@ -48,7 +48,7 @@
     mixed_ref, logsum_ref,
     x_v, wk_v, wv_v, wf_v, wrv_v, wrq_v, wq_v, wog_v, wao_v, wro_v,
     xn, kv, gates, q_t, m_s, l_s, acc, attn_t,
-    inner, vq, og, ext, st, chain_in, chain_out, incoming, part, mine, send2, recv1, recv2,
+    inner, vq, og, ext, st, chain_in, chain_out, incoming, part, send2, recv1, recv2,
     load_sem, col_send, row_send, recv_sem, st_send, st_recv, chain_send, chain_recv,
     s1_send, s1_recv, s2_send, s2_recv,
 ):
@@ -61,7 +61,8 @@
     chips = ntp // 2
     rb = rows // ntp
     pieces = rows // LANES
-    stride = rows + pieces * LANES
+    splits = s1_send.shape[1]
+    part_cols = width // splits
 
     sp, tp = lax.axis_index("sp"), lax.axis_index("tp")
     z, y = sp // ny, sp % ny
@@ -74,7 +75,9 @@
         (wrq_hbm, wrq_v), (wq_hbm, wq_v), (wog_hbm, wog_v), (wao_hbm, wao_v), (wro_hbm, wro_v),
     )):
         loads.append(pltpu.make_async_copy(src, dst, load_sem.at[i]))
-        loads[-1].start()
+
+    for copy in loads[:3]:
+        copy.start()
 
     barrier = pltpu.get_barrier_semaphore()
 
@@ -96,6 +99,8 @@
         greet((sp, ((chip + k) % chips) * 2 + core))
 
     loads[0].wait()
+    for copy in loads[3:6]:
+        copy.start()
     xf = x_v[...].astype(F32)
     scale = lax.rsqrt(jnp.mean(xf * xf, axis=-1, keepdims=True) + EPSILON)
     xn[...] = (xf * scale * in_gain[...]).astype(BF16)
@@ -113,50 +118,68 @@
     loads[1].wait()
     keys = head_norm(dot(xn[...], wk_v[...]), k_gain).astype(BF16)
     loads[2].wait()
+    for copy in loads[6:]:
+        copy.start()
     values_t = dot(xn[...], wv_v[...]).T.astype(BF16)
     for p in range(pairs):
         lanes = slice(p * LANES, (p + 1) * LANES)
-        kv[sp, p * stride : p * stride + rows, :] = keys[:, lanes]
+        kv[sp, 2 * p] = keys[:, lanes]
         for i in range(pieces):
-            at = p * stride + rows + i * LANES
-            kv[sp, at : at + LANES, :] = values_t[lanes, i * LANES : (i + 1) * LANES]
+            kv[sp, 2 * p + 1, i * LANES : (i + 1) * LANES, :] = values_t[
+                lanes, i * LANES : (i + 1) * LANES
+            ]
     gates[sp] = jnp.zeros((8, rows), F32)
     gates[sp, 0:heads, :] = gate_t[...]
 
-    def kv_copies(slot, send_sems, where):
-        return [
-            pltpu.make_async_remote_copy(
-                src_ref=buf.at[slot], dst_ref=buf.at[slot], send_sem=send_sems.at[i],
-                recv_sem=recv_sem.at[slot, i], device_id=where, device_id_type=MESH,
-            )
-            for i, buf in enumerate((gates, kv))
-        ]
-
-    def up_copies(source_z):
-        return kv_copies(source_z * ny + y, col_send.at[source_z], (sp + ny, tp))
-
-    def side_copies(source_z, k):
-        return kv_copies(
-            source_z * ny + y, row_send.at[source_z, k], (z * ny + (y + k) % ny, tp)
+    def piece(slot, i):
+        return gates.at[slot] if i == 0 else kv.at[slot, i - 1]
+
+    def piece_copy(slot, i, send, where):
+        return pltpu.make_async_remote_copy(
+            src_ref=piece(slot, i), dst_ref=piece(slot, i), send_sem=send.at[i],
+            recv_sem=recv_sem.at[slot, i], device_id=where, device_id_type=MESH,
         )
 
-    def wait_block(slot):
-        for copy in kv_copies(slot, col_send.at[0], (sp, partner)):
-            copy.wait_recv()
+    every = range(1 + 2 * pairs)
+
+    def pieces_of(p):
+        return ((0,) if p == 0 else ()) + (1 + 2 * p, 2 + 2 * p)
+
+    def up_copy(source_z, i):
+        return piece_copy(source_z * ny + y, i, col_send.at[source_z], (sp + ny, tp))
+
+    def side_copy(source_z, k, i):
+        where = (z * ny + (y + k) % ny, tp)
+        return piece_copy(source_z * ny + y, i, row_send.at[source_z, k], where)
+
+    def wait_pieces(slot, which):
+        for i in which:
+            piece_copy(slot, i, col_send.at[0], (sp, partner)).wait_recv()
+
+    def pass_on(source_z, p):
+        for i in pieces_of(p):
+            wait_pieces(source_z * ny + y, (i,))
+
+            @pl.when(z < nz - 1)
+            def _():
+                up_copy(source_z, i).start()
+
+            for k in range(1, ny):
+                side_copy(source_z, k, i).start()
 
     greeted = (ny - 1) + chips + (z > 0).astype(jnp.int32) + (z < nz - 1).astype(jnp.int32)
     pl.semaphore_wait(barrier, greeted)
 
     @pl.when(z < nz - 1)
     def _():
-        for copy in up_copies(z):
-            copy.start()
+        for i in every:
+            up_copy(z, i).start()
 
     for k in range(1, ny):
         @pl.when(y + k < ny)
         def _():
-            for copy in side_copies(z, k):
-                copy.start()
+            for i in every:
+                side_copy(z, k, i).start()
 
     tri = (iota((rows, rows), 0) >= iota((rows, rows), 1)).astype(F32)
     loads[3].wait()
@@ -204,6 +227,11 @@
     for k in range(1, ny):
         st_copy(k).start()
 
+    @pl.when(z > 0)
+    def _():
+        for p in range(pairs):
+            pass_on(z - 1, p)
+
     loads[6].wait()
     queries_t = (head_norm(dot(xn[...], wq_v[...]), q_gain).astype(BF16).astype(F32)).T
     half_of = iota((LANES, rows), 0) // HEAD_DIM
@@ -211,11 +239,10 @@
         pair = queries_t[(h // 2) * LANES : (h // 2 + 1) * LANES, :] * HEAD_DIM ** (-0.5)
         q_t[h] = jnp.where(half_of == h % 2, pair, 0.0).astype(BF16)
 
-    def attend(slot, own):
+    def attend(slot, p, own):
         gate = gates[slot].T
-        for h in range(heads):
-            base = (h // 2) * stride
-            s = dot(kv[slot, base : base + rows, :], q_t[h]) - gate[:, h : h + 1]
+        for h in (2 * p, 2 * p + 1):
+            s = dot(kv[slot, 2 * p], q_t[h]) - gate[:, h : h + 1]
             if own:
                 s = jnp.where(iota((rows, rows), 0) <= iota((rows, rows), 1), s, -jnp.inf)
                 top = jnp.max(s, axis=0, keepdims=True)
@@ -223,9 +250,11 @@
                 top = jnp.maximum(m_s[h], jnp.max(s, axis=0, keepdims=True))
             weights = jnp.exp(s - top)
             total = jnp.sum(weights, axis=0, keepdims=True)
-            at = base + rows + (h % 2) * HEAD_DIM
             v_t = jnp.concatenate(
-                [kv[slot, at + i * LANES : at + i * LANES + HEAD_DIM, :] for i in range(pieces)],
+                [
+                    kv[slot, 2 * p + 1, pl.ds(i * LANES + (h % 2) * HEAD_DIM, HEAD_DIM), :]
+                    for i in range(pieces)
+                ],
                 axis=1,
             )
             summed = dot(v_t, weights.astype(BF16))
@@ -238,7 +267,8 @@
                 acc[h] = acc[h] * fade + summed
             m_s[h] = top
 
-    attend(sp, True)
+    for p in range(pairs):
+        attend(sp, p, True)
 
     loads[7].wait()
     gate_out = dot(xn[...], wog_v[...])
@@ -279,39 +309,35 @@
         chain_in[...] = jnp.zeros_like(chain_in)
         advance_chain()
 
-    for k in range(1, ny):
-        @pl.when(y - k >= 0)
-        def _():
-            wait_block(sp - k)
-            attend(sp - k, False)
+    def attend_beside(d):
+        for k in range(1, ny):
+            other = (y + k) % ny
+
+            @pl.when((d > 0) | (other < y))
+            def _():
+                slot = (z - d) * ny + other
+                for p in range(pairs):
+                    wait_pieces(slot, pieces_of(p))
+                    attend(slot, p, False)
 
     def step(d, carry):
-        source = z - d
-        wait_block(source * ny + y)
-
-        @pl.when(z < nz - 1)
-        def _():
-            for copy in up_copies(source):
-                copy.start()
-
-        for k in range(1, ny):
-            for copy in side_copies(source, k):
-                copy.start()
-
-        attend(source * ny + y, False)
+        for p in range(pairs):
+            @pl.when(d < z)
+            def _():
+                pass_on(z - d - 1, p)
+
+            attend((z - d) * ny + y, p, False)
 
         @pl.when(d == jnp.maximum(z - 1, 1))
         def _():
             chain_copy.wait_recv()
             advance_chain()
 
-        for k in range(1, ny):
-            slot = source * ny + (y + k) % ny
-            wait_block(slot)
-            attend(slot, False)
+        attend_beside(d - 1)
         return carry
 
     lax.fori_loop(1, z + 1, step, 0)
+    attend_beside(z)
 
     for h in range(heads):
         mixed = acc[h] / l_s[h]
@@ -327,69 +353,88 @@
         vq[:, lanes] = out.astype(BF16)
     loads[8].wait()
     loads[9].wait()
-    part[...] = (dot(attn_out, wao_v[...]) + dot(vq[...], wro_v[...])).astype(BF16)
 
     def rows_of(which_chip, which_core):
         return pl.ds(pl.multiple_of((which_chip * 2 + which_core) * rb, rb), rb)
 
-    def within(j):
+    def columns(q):
+        return slice(q * part_cols, (q + 1) * part_cols)
+
+    def within(j, q):
         return pltpu.make_async_remote_copy(
-            src_ref=part.at[rows_of(j, 1 - core)], dst_ref=recv1.at[j], send_sem=s1_send.at[j],
-            recv_sem=s1_recv.at[j], device_id=(sp, partner), device_id_type=MESH,
+            src_ref=part.at[q, rows_of(j, 1 - core)], dst_ref=recv1.at[j, q],
+            send_sem=s1_send.at[j, q], recv_sem=s1_recv.at[j, q], device_id=(sp, partner),
+            device_id_type=MESH,
         )
 
-    def between(j):
+    def between(j, q):
         return pltpu.make_async_remote_copy(
-            src_ref=send2.at[j], dst_ref=recv2.at[chip], send_sem=s2_send.at[j],
-            recv_sem=s2_recv.at[chip], device_id=(sp, j * 2 + core), device_id_type=MESH,
+            src_ref=send2.at[j, q], dst_ref=recv2.at[chip, q], send_sem=s2_send.at[j, q],
+            recv_sem=s2_recv.at[chip, q], device_id=(sp, j * 2 + core), device_id_type=MESH,
         )
 
-    order = [(chip + k) % chips for k in range(1, chips)] + [chip]
-    for j in order:
-        within(j).start()
-    for j in order[:-1]:
-        within(j).wait_recv()
-        send2[j] = (part[rows_of(j, core), :].astype(F32) + recv1[j].astype(F32)).astype(BF16)
-        between(j).start()
-    within(chip).wait_recv()
-    mine[...] = part[rows_of(chip, core), :].astype(F32) + recv1[chip].astype(F32)
-    for j in order[:-1]:
-        pltpu.make_async_remote_copy(
-            src_ref=send2.at[j], dst_ref=recv2.at[j], send_sem=s2_send.at[j],
-            recv_sem=s2_recv.at[j], device_id=(sp, partner), device_id_type=MESH,
-        ).wait_recv()
-        mine[...] += recv2[j].astype(F32)
-    mixed_ref[...] = mine[...].astype(BF16)
-
-    for j in order:
-        within(j).wait_send()
-    for j in order[:-1]:
-        between(j).wait_send()
+    order = [(chip + k) % chips for k in range(1, chips)]
+
+    def chip_sum(j, q):
+        within(j, q).wait_recv()
+        return part[q, rows_of(j, core), :].astype(F32) + recv1[j, q].astype(F32)
+
+    def send_sums(q):
+        for j in order:
+            send2[j, q] = chip_sum(j, q).astype(BF16)
+            between(j, q).start()
+
+    for q in range(splits):
+        part[q] = (
+            dot(attn_out, wao_v[:, columns(q)]) + dot(vq[...], wro_v[:, columns(q)])
+        ).astype(BF16)
+        for j in order:
+            within(j, q).start()
+        if q > 0:
+            send_sums(q - 1)
+    send_sums(splits - 1)
+    for q in range(splits):
+        within(chip, q).start()
+    for q in range(splits):
+        total = chip_sum(chip, q)
+        for j in order:
+            pltpu.make_async_remote_copy(
+                src_ref=send2.at[j, q], dst_ref=recv2.at[j, q], send_sem=s2_send.at[j, q],
+                recv_sem=s2_recv.at[j, q], device_id=(sp, partner), device_id_type=MESH,
+            ).wait_recv()
+            total = total + recv2[j, q].astype(F32)
+        mixed_ref[:, columns(q)] = total.astype(BF16)
+
+    for q in range(splits):
+        for j in order + [chip]:
+            within(j, q).wait_send()
+        for j in order:
+            between(j, q).wait_send()
     for k in range(1, ny):
         st_copy(k).wait_send()
 
         @pl.when(y + k < ny)
         def _():
-            for copy in side_copies(z, k):
-                copy.wait_send()
+            for i in every:
+                side_copy(z, k, i).wait_send()
 
     @pl.when(z < nz - 1)
     def _():
         chain_copy.wait_send()
-        for copy in up_copies(z):
-            copy.wait_send()
+        for i in every:
+            up_copy(z, i).wait_send()
 
     def drain(d, carry):
         source = z - d
 
         @pl.when(z < nz - 1)
         def _():
-            for copy in up_copies(source):
-                copy.wait_send()
+            for i in every:
+                up_copy(source, i).wait_send()
 
         for k in range(1, ny):
-            for copy in side_copies(source, k):
-                copy.wait_send()
+            for i in every:
+                side_copy(source, k, i).wait_send()
         return carry
 
     lax.fori_loop(1, z + 1, drain, 0)
@@ -407,6 +452,7 @@
     cols = query_weight.shape[1]
     heads, pairs, rec_heads = cols // HEAD_DIM, cols // LANES, cols // STATE_ROWS
     rb, chips = rows // n_tp, n_tp // 2
+    kinds, splits = 1 + 2 * pairs, math.gcd(width // LANES, 4)
     weight = pltpu.VMEM((width, cols), BF16)
     out_weight = pltpu.VMEM((cols, width), BF16)
     dma = pltpu.SemaphoreType.DMA
@@ -425,7 +471,7 @@
             pltpu.VMEM((rows, width), BF16),
             *([weight] * 7), out_weight, out_weight,
             pltpu.VMEM((rows, width), BF16),
-            pltpu.VMEM((n_sp, pairs * 2 * rows, LANES), BF16),
+            pltpu.VMEM((n_sp, 2 * pairs, rows, LANES), BF16),
             pltpu.VMEM((n_sp, 8, rows), F32),
             pltpu.VMEM((heads, LANES, rows), BF16),
             pltpu.VMEM((heads, 1, rows), F32),
@@ -440,15 +486,12 @@
             pltpu.VMEM((cols, STATE_ROWS), BF16),
             pltpu.VMEM((cols, STATE_ROWS), BF16),
             pltpu.VMEM((cols, STATE_ROWS), BF16),
-            pltpu.VMEM((rows, width), BF16),
-            pltpu.VMEM((rb, width), F32),
-            pltpu.VMEM((chips, rb, width), BF16),
-            pltpu.VMEM((chips, rb, width), BF16),
-            pltpu.VMEM((chips, rb, width), BF16),
+            pltpu.VMEM((splits, rows, width // splits), BF16),
+            *([pltpu.VMEM((chips, splits, rb, width // splits), BF16)] * 3),
             dma((10,)),
-            dma((nz, 2)), dma((nz, ny, 2)), dma((n_sp, 2)),
+            dma((nz, kinds)), dma((nz, ny, kinds)), dma((n_sp, kinds)),
             dma((ny,)), dma((ny,)), dma, dma,
-            dma((chips,)), dma((chips,)), dma((chips,)), dma((chips,)),
+            *([dma((chips, splits))] * 4),
         ],
         compiler_params=pltpu.CompilerParams(
             collective_id=0, has_side_effects=True, vmem_limit_bytes=60 * 1024 * 1024

time: 50.6 us -> 45.7 us (0.903)
  the two profiles are of different devices: /device:TPU:25 before, /device:TPU:29 now
where the time goes in v2:
time: 45.7 us; the launch traced here: 45.6 us
  Pallas kernels  42.6 us (93%)
  local copies, waits for them, and re-layouts  2.27 us (5%)
  between operations  0.65 us (1%)
    pallas_call x1, Pallas kernels, body(): pl.pallas_call(functools.partial(kernel, (nz, ny, n_tp)), name='mixer', o...  42.6 us
    unnamed x4, local copies, waits for them, and re-layouts  2.27 us

profile of v2, /device:TPU:29, one launch (start us, length us, event | category | flops | bytes accessed | tf_op | source)
XLA Modules:
  0.0 45.6 jit_solution(8884723096957454307)
XLA Ops:
  0.6 42.6 %mixer.1 = (bf16[64,2048]{1,0:T(8,128)(2,1)}, f32[4,256]{1,0:T(4,128)}) custom-call(bf16[256,2048]{1,0:T(8,128)(2,1)} %x_hbm.1, bf16[2048,256]{1,0:T(8,128)(2,1)} %wk_hbm.1, bf16[2048,256]{1,0:T(8,128)(2,1)} %wv_hbm.1, bf16[2048,256]{1,0:T(8,128)(2,1)} %wf_hbm.1, bf16[2048,256]{1,0:T(8,128)(2,1)} %wrv_hbm.1, bf16[2048,256]{1,0:T(8,128)(2,1)} %wrq_hbm.1, ...), custom_call_target="tpu_custom_call" | custom-call | tf_op jit(solution)/shard_map/mixer/pallas_call | solution.py:461
  43.3 0.0 copy-start
  43.3 1.7 %copy.22 = bf16[64,2048]{1,0:T(8,128)(2,1)} copy(bf16[64,2048]{1,0:T(8,128)(2,1)} %get-tuple-element.8) | data formatting | bytes 524288
  45.0 0.0 copy-done
  45.0 0.6 %copy.23 = f32[256,4]{0,1:T(4,128)} copy(f32[256,4]{0,1:T(4,128)S(1)} %bitcast.11) | data formatting | bytes 8192
Async XLA Ops:
  43.3 1.7 %copy-start = (f32[4,256]{1,0:T(4,128)S(1)}, f32[4,256]{1,0:T(4,128)}, u32[]{:S(2)}) copy-start(f32[4,256]{1,0:T(4,128)} %get-tuple-element.5) | copy-start | bytes 12292

commit v3 on v2

--- a/solution.py
+++ b/solution.py
@@ -44,11 +44,13 @@
 def kernel(
     sizes,
     x_hbm, wk_hbm, wv_hbm, wf_hbm, wrv_hbm, wrq_hbm, wq_hbm, wog_hbm, wao_hbm, wro_hbm,
-    in_gain, q_gain, k_gain, gate_t, a_gain, slack, extra_t, r_gain,
+    in_gain_hbm, q_gain_hbm, k_gain_hbm, gate_t_hbm, a_gain_hbm,
+    slack_hbm, extra_t_hbm, r_gain_hbm,
     mixed_ref, logsum_ref,
     x_v, wk_v, wv_v, wf_v, wrv_v, wrq_v, wq_v, wog_v, wao_v, wro_v,
     xn, kv, gates, q_t, m_s, l_s, acc, attn_t,
     inner, vq, og, ext, st, chain_in, chain_out, incoming, part, send2, recv1, recv2,
+    in_gain, q_gain, k_gain, gate_t, a_gain, slack, extra_t, r_gain, rec_part,
     load_sem, col_send, row_send, recv_sem, st_send, st_recv, chain_send, chain_recv,
     s1_send, s1_recv, s2_send, s2_recv,
 ):
@@ -73,10 +75,13 @@
     for i, (src, dst) in enumerate((
         (x_hbm, x_v), (wk_hbm, wk_v), (wv_hbm, wv_v), (wf_hbm, wf_v), (wrv_hbm, wrv_v),
         (wrq_hbm, wrq_v), (wq_hbm, wq_v), (wog_hbm, wog_v), (wao_hbm, wao_v), (wro_hbm, wro_v),
+        (in_gain_hbm, in_gain), (q_gain_hbm, q_gain), (k_gain_hbm, k_gain),
+        (gate_t_hbm, gate_t), (a_gain_hbm, a_gain), (slack_hbm, slack),
+        (extra_t_hbm, extra_t), (r_gain_hbm, r_gain),
     )):
         loads.append(pltpu.make_async_copy(src, dst, load_sem.at[i]))
 
-    for copy in loads[:3]:
+    for copy in loads[:3] + loads[10:]:
         copy.start()
 
     barrier = pltpu.get_barrier_semaphore()
@@ -99,6 +104,8 @@
         greet((sp, ((chip + k) % chips) * 2 + core))
 
     loads[0].wait()
+    for copy in loads[10:]:
+        copy.wait()
     for copy in loads[3:6]:
         copy.start()
     xf = x_v[...].astype(F32)
@@ -117,17 +124,8 @@
 
     loads[1].wait()
     keys = head_norm(dot(xn[...], wk_v[...]), k_gain).astype(BF16)
-    loads[2].wait()
-    for copy in loads[6:]:
-        copy.start()
-    values_t = dot(xn[...], wv_v[...]).T.astype(BF16)
     for p in range(pairs):
-        lanes = slice(p * LANES, (p + 1) * LANES)
-        kv[sp, 2 * p] = keys[:, lanes]
-        for i in range(pieces):
-            kv[sp, 2 * p + 1, i * LANES : (i + 1) * LANES, :] = values_t[
-                lanes, i * LANES : (i + 1) * LANES
-            ]
+        kv[sp, 2 * p] = keys[:, p * LANES : (p + 1) * LANES]
     gates[sp] = jnp.zeros((8, rows), F32)
     gates[sp, 0:heads, :] = gate_t[...]
 
@@ -170,16 +168,30 @@
     greeted = (ny - 1) + chips + (z > 0).astype(jnp.int32) + (z < nz - 1).astype(jnp.int32)
     pl.semaphore_wait(barrier, greeted)
 
-    @pl.when(z < nz - 1)
-    def _():
-        for i in every:
-            up_copy(z, i).start()
-
-    for k in range(1, ny):
-        @pl.when(y + k < ny)
+    def start_own(which):
+        @pl.when(z < nz - 1)
         def _():
-            for i in every:
-                side_copy(z, k, i).start()
+            for i in which:
+                up_copy(z, i).start()
+
+        for k in range(1, ny):
+            @pl.when(y + k < ny)
+            def _():
+                for i in which:
+                    side_copy(z, k, i).start()
+
+    start_own([0] + [1 + 2 * p for p in range(pairs)])
+
+    loads[2].wait()
+    for copy in loads[6:10]:
+        copy.start()
+    values_t = dot(xn[...], wv_v[...]).T.astype(BF16)
+    for p in range(pairs):
+        for i in range(pieces):
+            kv[sp, 2 * p + 1, i * LANES : (i + 1) * LANES, :] = values_t[
+                p * LANES : (p + 1) * LANES, i * LANES : (i + 1) * LANES
+            ]
+    start_own([2 + 2 * p for p in range(pairs)])
 
     tri = (iota((rows, rows), 0) >= iota((rows, rows), 1)).astype(F32)
     loads[3].wait()
@@ -337,6 +349,15 @@
         return carry
 
     lax.fori_loop(1, z + 1, step, 0)
+    for j in range(rec_heads):
+        lanes = slice(j * STATE_ROWS, (j + 1) * STATE_ROWS)
+        out = inner[:, lanes] + dot_nt(vq[:, lanes], incoming[lanes, :])
+        mean = jnp.mean(out * out, axis=-1, keepdims=True)
+        out = out * lax.rsqrt(mean + EPSILON) * r_gain[:, lanes] * og[:, lanes]
+        vq[:, lanes] = out.astype(BF16)
+    loads[9].wait()
+    rec_part[...] = dot(vq[...], wro_v[...])
+
     attend_beside(z)
 
     for h in range(heads):
@@ -345,14 +366,7 @@
         attn_t[h * HEAD_DIM : (h + 1) * HEAD_DIM, :] = mixed * lax.rsqrt(mean + EPSILON)
         logsum_ref[h : h + 1, :] = m_s[h] + jnp.log(l_s[h]) + gate_t[h : h + 1, :]
     attn_out = (attn_t[...].T * a_gain[...]).astype(BF16)
-    for j in range(rec_heads):
-        lanes = slice(j * STATE_ROWS, (j + 1) * STATE_ROWS)
-        out = inner[:, lanes] + dot_nt(vq[:, lanes], incoming[lanes, :])
-        mean = jnp.mean(out * out, axis=-1, keepdims=True)
-        out = out * lax.rsqrt(mean + EPSILON) * r_gain[:, lanes] * og[:, lanes]
-        vq[:, lanes] = out.astype(BF16)
     loads[8].wait()
-    loads[9].wait()
 
     def rows_of(which_chip, which_core):
         return pl.ds(pl.multiple_of((which_chip * 2 + which_core) * rb, rb), rb)
@@ -386,7 +400,7 @@
 
     for q in range(splits):
         part[q] = (
-            dot(attn_out, wao_v[:, columns(q)]) + dot(vq[...], wro_v[:, columns(q)])
+            dot(attn_out, wao_v[:, columns(q)]) + rec_part[:, columns(q)]
         ).astype(BF16)
         for j in order:
             within(j, q).start()
@@ -465,7 +479,7 @@
             jax.ShapeDtypeStruct((rb, width), BF16),
             jax.ShapeDtypeStruct((heads, rows), F32),
         ),
-        in_specs=[any_space] * 10 + [vmem] * 8,
+        in_specs=[any_space] * 18,
         out_specs=(vmem, vmem),
         scratch_shapes=[
             pltpu.VMEM((rows, width), BF16),
@@ -488,7 +502,14 @@
             pltpu.VMEM((cols, STATE_ROWS), BF16),
             pltpu.VMEM((splits, rows, width // splits), BF16),
             *([pltpu.VMEM((chips, splits, rb, width // splits), BF16)] * 3),
-            dma((10,)),
+            *([pltpu.VMEM((1, n), F32) for n in (width, HEAD_DIM, HEAD_DIM)]),
+            pltpu.VMEM((heads, rows), F32),
+            pltpu.VMEM((1, cols), F32),
+            pltpu.VMEM((1, cols), F32),
+            pltpu.VMEM((rec_heads, rows), F32),
+            pltpu.VMEM((1, cols), F32),
+            pltpu.VMEM((rows, width), F32),
+            dma((18,)),
             dma((nz, kinds)), dma((nz, ny, kinds)), dma((n_sp, kinds)),
             dma((ny,)), dma((ny,)), dma, dma,
             *([dma((chips, splits))] * 4),

time: 45.7 us -> 44.4 us (0.972)
  Pallas kernels: 42.6 us -> 41.3 us
    pallas_call x1, Pallas kernels: 42.6 us -> 41.3 us  [body(): pl.pallas_call(functools.partial(kernel, (nz, ny, n_tp)), name='mixer', o...]
where the time goes in v3:
time: 44.4 us; the launch traced here: 44.2 us
  Pallas kernels  41.3 us (93%)
  local copies, waits for them, and re-layouts  2.27 us (5%)
  between operations  0.65 us (1%)
    pallas_call x1, Pallas kernels, body(): pl.pallas_call(functools.partial(kernel, (nz, ny, n_tp)), name='mixer', o...  41.3 us
    unnamed x4, local copies, waits for them, and re-layouts  2.27 us

profile of v3, /device:TPU:29, one launch (start us, length us, event | category | flops | bytes accessed | tf_op | source)
XLA Modules:
  0.0 44.2 jit_solution(9758621611723256476)
XLA Ops:
  0.6 41.3 %mixer.1 = (bf16[64,2048]{1,0:T(8,128)(2,1)}, f32[4,256]{1,0:T(4,128)}) custom-call(bf16[256,2048]{1,0:T(8,128)(2,1)} %x_hbm.1, bf16[2048,256]{1,0:T(8,128)(2,1)} %wk_hbm.1, bf16[2048,256]{1,0:T(8,128)(2,1)} %wv_hbm.1, bf16[2048,256]{1,0:T(8,128)(2,1)} %wf_hbm.1, bf16[2048,256]{1,0:T(8,128)(2,1)} %wrv_hbm.1, bf16[2048,256]{1,0:T(8,128)(2,1)} %wrq_hbm.1, ...), custom_call_target="tpu_custom_call" | custom-call | tf_op jit(solution)/shard_map/mixer/pallas_call | solution.py:475
  41.9 0.0 copy-start
  41.9 1.7 %copy.22 = bf16[64,2048]{1,0:T(8,128)(2,1)} copy(bf16[64,2048]{1,0:T(8,128)(2,1)} %get-tuple-element.8) | data formatting | bytes 524288
  43.6 0.0 copy-done
  43.6 0.6 %copy.23 = f32[256,4]{0,1:T(4,128)} copy(f32[256,4]{0,1:T(4,128)S(1)} %bitcast.11) | data formatting | bytes 8192
Async XLA Ops:
  41.9 1.7 %copy-start = (f32[4,256]{1,0:T(4,128)S(1)}, f32[4,256]{1,0:T(4,128)}, u32[]{:S(2)}) copy-start(f32[4,256]{1,0:T(4,128)} %get-tuple-element.5) | copy-start | bytes 12292
